TPU v7x, 32 devices: a whole 2x2x4 slice. The times are simulated.
32 devices in a mesh: grp: 2 (over y), ra: 4 (over z), cb: 4 (over x, core).
Axes of the slice: x: 2, y: 2, z: 4, core: 2. Of those that a mesh axis runs over, the one named last changes fastest.
Arguments:
- tokens: bfloat16 [256, 4096], P('grp', 'ra'), parts along dimension 0, may hold values from -20 to 20
- norm_gain: float32 [4096], P('ra'), may hold values from 0.1 to 1.9
- gate_weight: float32 [4096, 11264], P('ra', 'cb'), may hold values from -0.09375 to 0.09375
- gate_scale: float32 [11264], P('cb'), may hold values from 0.5 to 2
- up_weight: float32 [4096, 11264], P('ra', 'cb'), may hold values from -0.09375 to 0.09375
- up_scale: float32 [11264], P('cb'), may hold values from 0.5 to 2
- down_weight: float32 [11264, 4096], P('cb', 'ra'), may hold values from -1 to 1
- down_scale: float32 [4096], P('ra'), may hold values from 0.5 to 2
- out_gain: float32 [4096], P('ra'), may hold values from 0.1 to 1.9
Outputs:
- normed: bfloat16 [256, 4096], P('grp', 'ra'), parts along dimension 0
There are 2 independent parts, one for each index of `grp`. A program takes and returns all parts, laid end to end along the dimension named above; an argument that names none is the same for every part. Nothing has to cross between parts.
All inputs are finite; a program needn't handle non-finite values.
Results may differ from a plain program's by a relative error of at most 0.012.
Values may be sent and summed in bfloat16 or wider, within the bound.
A program may use at most 64 MiB of HBM per device.

v0:
```python
import jax
import jax.numpy as jnp
from jax import lax
from jax.sharding import PartitionSpec as P


def on_device(
    tokens,
    norm_gain,
    gate_weight,
    gate_scale,
    up_weight,
    up_scale,
    down_weight,
    down_scale,
    out_gain,
):
    width = tokens.shape[1] * lax.axis_size("ra")
    values = tokens.astype(jnp.float32)
    squares = lax.psum(jnp.sum(values * values, axis=1), "ra")
    inv_first = lax.rsqrt(squares / width + 1e-06)[:, None]
    normed_in = (values * inv_first * norm_gain).astype(jnp.bfloat16)
    gate_local = gate_weight.astype(jnp.bfloat16)
    up_local = up_weight.astype(jnp.bfloat16)
    down_local = down_weight.astype(jnp.bfloat16)
    gate_part = jnp.dot(normed_in, gate_local, preferred_element_type=jnp.float32)
    up_part = jnp.dot(normed_in, up_local, preferred_element_type=jnp.float32)
    gate, up = (
        lax.psum_scatter(gate_part, "ra", scatter_dimension=1, tiled=True),
        lax.psum_scatter(up_part, "ra", scatter_dimension=1, tiled=True),
    )
    share = gate.shape[1]
    offset = lax.axis_index("ra") * share
    gate_cols = lax.dynamic_slice_in_dim(gate_scale, offset, share, 0)
    up_cols = lax.dynamic_slice_in_dim(up_scale, offset, share, 0)
    hidden_share = (jax.nn.silu(gate * gate_cols) * (up * up_cols)).astype(jnp.bfloat16)
    partial_value = jnp.dot(
        lax.all_gather(hidden_share, "ra", axis=1, tiled=True),
        down_local,
        preferred_element_type=jnp.float32,
    )
    branch = lax.psum(partial_value, "cb") * down_scale
    mixed = 0.5 * values + branch
    second = lax.psum(jnp.sum(mixed * mixed, axis=1), "ra")
    inv_second = lax.rsqrt(second / width + 1e-06)[:, None]
    return (mixed * inv_second * out_gain).astype(jnp.bfloat16)


def solution(mesh):
    return jax.shard_map(
        on_device,
        mesh=mesh,
        in_specs=(
            P("grp", "ra"),
            P("ra"),
            P("ra", "cb"),
            P("cb"),
            P("ra", "cb"),
            P("cb"),
            P("cb", "ra"),
            P("ra"),
            P("ra"),
        ),
        out_specs=P("grp", "ra"),
        check_vma=False,
    )
```

profile of v0, /device:TPU:0, one launch (start us, length us, event | category | flops | bytes accessed | tf_op | source)
XLA Modules:
  0.0 173.9 jit_solution(2744904956569881373)
XLA Ops:
  6.5 0.0 reduce-scatter.5.cloned.1.call-start
  6.5 1.1 fusion.7
  7.6 13.5 %psum.21 = f32[128]{0:T(128)S(1)} all-reduce(f32[128]{0:T(128)S(1)} %fusion.7), channel_id=1, replica_groups=mesh['grp'=2,'ra'=4,'cb'=4] {'ra'}, use_global_device_ids=true, to_apply=%region_1.0 | all-reduce | flops 128 | bytes 1024 | tf_op jit(solution)/shard_map/psum | solution.py:20
  21.1 0.0 copy-start
  21.1 0.0 copy-start.1
  21.1 7.9 %fusion.2 = f32[128,2816]{0,1:T(8,128)} fusion(f32[1024,2816]{1,0:T(8,128)} %param.13, bf16[128,1024]{1,0:T(8,128)(2,1)} %param.9, f32[1024]{0:T(1024)} %param.10, f32[128]{0:T(128)S(1)} %add_rsqrt_fusion.1), kind=kOutput, calls=%fused_computation.2 | convolution fusion | flops 741605376 | bytes 13242880 | tf_op jit(solution)/shard_map/dot_general | solution.py:27
  29.1 0.0 reduce-scatter.5.cloned.1.call-update
  29.1 0.0 reduce-scatter.3.cloned.1.call-start
  29.1 0.0 copy-done
  29.1 0.0 copy-done.1
  29.2 7.8 %fusion.4 = f32[128,2816]{0,1:T(8,128)} fusion(f32[1024,2816]{1,0:T(8,128)} %param.11, bf16[128,1024]{1,0:T(8,128)(2,1)S(1)} %copy-done, f32[1024]{0:T(1024)S(1)} %copy-done.1, f32[128]{0:T(128)S(1)} %add_rsqrt_fusion.1), kind=kOutput, calls=%fused_computation.4 | convolution fusion | flops 741605376 | bytes 13242880 | tf_op jit(solution)/shard_map/dot_general | solution.py:26
  37.0 0.0 reduce-scatter.3.cloned.1.call-update
  37.0 0.0 all-reduce.2.cloned.1.call-start
  37.0 0.8 dynamic_slice.7
  37.8 0.8 dynamic_slice.6
  38.6 22.3 %reduce-scatter.5.cloned.1.call-done = f32[128,704]{0,1:T(8,128)} async-done(((f32[128,2816]{0,1:T(8,128)}), f32[128,704]{0,1:T(8,128)}) %reduce-scatter.5.cloned.1.call-update) | async-done | bytes 360464 | tf_op jit(solution)/shard_map/reduce_scatter | solution.py:30
  60.8 34.5 %reduce-scatter.3.cloned.1.call-done = f32[128,704]{0,1:T(8,128)} async-done(((f32[128,2816]{0,1:T(8,128)}), f32[128,704]{0,1:T(8,128)}) %reduce-scatter.3.cloned.1.call-update) | async-done | bytes 360464 | tf_op jit(solution)/shard_map/reduce_scatter | solution.py:29
  95.4 1.3 multiply_convert_fusion.1
  96.7 17.1 %all_gather.3 = bf16[128,2816]{0,1:T(8,128)(2,1)S(1)} all-gather(bf16[128,704]{0,1:T(8,128)(2,1)S(1)} %multiply_convert_fusion.1), channel_id=1, replica_groups=mesh['grp'=2,'ra'=4,'cb'=4] {'ra'}, dimensions={1}, use_global_device_ids=true | all-gather | bytes 901120 | tf_op jit(solution)/shard_map/all_gather | solution.py:38
  113.9 0.0 copy-start.2
  113.9 0.0 copy-start.3
  113.9 6.1 %fusion = f32[128,1024]{1,0:T(8,128)} fusion(bf16[128,2816]{0,1:T(8,128)(2,1)S(1)} %all_gather.3, f32[2816,1024]{1,0:T(8,128)} %param.15), kind=kOutput, calls=%fused_computation | convolution fusion | flops 741081088 | bytes 12779520 | tf_op jit(solution)/shard_map/dot_general | solution.py:37
  120.0 0.0 all-reduce.2.cloned.1.call-update
  120.0 32.6 %all-reduce.2.cloned.1.call-done = f32[128,1024]{1,0:T(8,128)} async-done(((f32[128,1024]{1,0:T(8,128)}), f32[128,1024]{1,0:T(8,128)}) %all-reduce.2.cloned.1.call-update) | async-done | bytes 524304 | tf_op jit(solution)/shard_map/psum | solution.py:42
  152.6 0.0 copy-done.2
  152.6 1.2 multiply_reduce_fusion
  153.8 11.7 %psum.23 = f32[128]{0:T(128)S(1)} all-reduce(f32[128]{0:T(128)S(1)} %multiply_reduce_fusion), channel_id=1, replica_groups=mesh['grp'=2,'ra'=4,'cb'=4] {'ra'}, use_global_device_ids=true, to_apply=%region_6.7 | all-reduce | flops 128 | bytes 1024 | tf_op jit(solution)/shard_map/psum | solution.py:44
  165.5 0.0 copy-done.3
  165.5 1.9 %multiply_convert_fusion = bf16[128,1024]{1,0:T(8,128)(2,1)} fusion(f32[128,1024]{1,0:T(8,128)} %all-reduce.2.cloned.1.call-done, bf16[128,1024]{1,0:T(8,128)(2,1)S(1)} %copy-done, f32[1024]{0:T(1024)S(1)} %copy-done.3, f32[128]{0:T(128)S(1)} %add_rsqrt_fusion, f32[1024]{0:T(1024)S(1)} %copy-done.2), kind=kLoop, calls=%fused_computation.13 | loop fusion | flops 917504 | bytes 1057280 | tf_op jit(solution)/shard_map/convert_element_type | solution.py:46
  (2 shorter events, 0.0 us)
Async XLA Ops:
  6.5 54.3 %reduce-scatter.5.cloned.1.call-start = ((), (), s32[]{:S(2)}) async-start(), calls=%async_computation.3 | async-start | bytes 1802240 | tf_op jit(solution)/shard_map/reduce_scatter | solution.py:30
  21.1 8.0 %copy-start = (bf16[128,1024]{1,0:T(8,128)(2,1)S(1)}, bf16[128,1024]{1,0:T(8,128)(2,1)}, u32[]{:S(2)}) copy-start(bf16[128,1024]{1,0:T(8,128)(2,1)} %param.9) | copy-start | bytes 786436
  21.1 8.0 %copy-start.1 = (f32[1024]{0:T(1024)S(1)}, f32[1024]{0:T(1024)}, u32[]{:S(2)}) copy-start(f32[1024]{0:T(1024)} %param.10) | copy-start | bytes 12292
  29.1 66.3 %reduce-scatter.3.cloned.1.call-start = ((), (), s32[]{:S(2)}) async-start(), calls=%async_computation.2 | async-start | bytes 1802240 | tf_op jit(solution)/shard_map/reduce_scatter | solution.py:29
  37.0 115.6 %all-reduce.2.cloned.1.call-start = ((), (), s32[]{:S(2)}) async-start(), calls=%async_computation.4 | async-start | bytes 1048576 | tf_op jit(solution)/shard_map/psum | solution.py:42
  113.9 38.7 %copy-start.2 = (f32[1024]{0:T(1024)S(1)}, f32[1024]{0:T(1024)}, u32[]{:S(2)}) copy-start(f32[1024]{0:T(1024)} %param.16) | copy-start | bytes 12292
  113.9 51.6 %copy-start.3 = (f32[1024]{0:T(1024)S(1)}, f32[1024]{0:T(1024)}, u32[]{:S(2)}) copy-start(f32[1024]{0:T(1024)} %param.17) | copy-start | bytes 12292
Sparse Core Ops, SparseCore 0:
  29.2 31.5 reduce-scatter.4
  63.2 32.1 reduce-scatter.2
  120.1 32.4 all-reduce.1
where the time goes:
time: 174 us
  waiting for transfers between devices  89.4 us (51%)
  blocking collectives  42.3 us (24%)
  matrix products  21.8 us (13%)
  between operations  13.1 us (8%)
  other arithmetic  5.53 us (3%)
    reduce_scatter x1, waiting for transfers between devices, on_device(): lax.psum_scatter(gate_part, 'ra', scatter_dimension=1, tiled=True)  34.5 us
    psum x1, waiting for transfers between devices, on_device(): branch = lax.psum(partial_value, 'cb') * down_scale  32.6 us
    reduce_scatter x1, waiting for transfers between devices, on_device(): lax.psum_scatter(up_part, 'ra', scatter_dimension=1, tiled=True)  22.3 us
    all_gather x1, blocking collectives, on_device(): lax.all_gather(hidden_share, 'ra', axis=1, tiled=True)  17.1 us
    psum x1, blocking collectives, on_device(): squares = lax.psum(jnp.sum(values * values, axis=1), 'ra')  13.5 us
    psum x1, blocking collectives, on_device(): second = lax.psum(jnp.sum(mixed * mixed, axis=1), 'ra')  11.7 us
    dot_general x1, matrix products, on_device(): up_part = jnp.dot(normed_in, up_local, preferred_element_type=jnp.float32)  7.94 us
    dot_general x1, matrix products, on_device(): jnp.dot(normed_in, gate_local, preferred_element_type=jnp.float32)  7.8 us
  transfers between devices with their start and end apart: 3, of which 3 were waited for; matrix products, arithmetic and copies ran while one was open for 5% of the time, Pallas kernels for 0%

commit v1 on v0

v1 whole, which is shorter than its diff:
```python
import functools

import jax
import jax.numpy as jnp
from jax import lax
from jax.experimental import pallas as pl
from jax.experimental.pallas import tpu as pltpu
from jax.sharding import PartitionSpec as P

MESH = pl.DeviceIdType.MESH
F32 = jnp.float32
BF16 = jnp.bfloat16


def plain(tokens, norm_gain, gate_weight, gate_scale, up_weight, up_scale, down_weight, down_scale, out_gain):
    width = tokens.shape[1] * lax.axis_size("ra")
    values = tokens.astype(F32)
    squares = lax.psum(jnp.sum(values * values, axis=1), "ra")
    inv_first = lax.rsqrt(squares / width + 1e-06)[:, None]
    normed_in = (values * inv_first * norm_gain).astype(BF16)
    gate_part = jnp.dot(normed_in, gate_weight.astype(BF16), preferred_element_type=F32)
    up_part = jnp.dot(normed_in, up_weight.astype(BF16), preferred_element_type=F32)
    gate = lax.psum_scatter(gate_part, "ra", scatter_dimension=1, tiled=True)
    up = lax.psum_scatter(up_part, "ra", scatter_dimension=1, tiled=True)
    share = gate.shape[1]
    offset = lax.axis_index("ra") * share
    gate_cols = lax.dynamic_slice_in_dim(gate_scale, offset, share, 0)
    up_cols = lax.dynamic_slice_in_dim(up_scale, offset, share, 0)
    hidden_share = (jax.nn.silu(gate * gate_cols) * (up * up_cols)).astype(BF16)
    partial_value = jnp.dot(
        lax.all_gather(hidden_share, "ra", axis=1, tiled=True),
        down_weight.astype(BF16),
        preferred_element_type=F32,
    )
    branch = lax.psum(partial_value, "cb") * down_scale
    mixed = 0.5 * values + branch
    second = lax.psum(jnp.sum(mixed * mixed, axis=1), "ra")
    inv_second = lax.rsqrt(second / width + 1e-06)[:, None]
    return (mixed * inv_second * out_gain).astype(BF16)


def diagonal(rows, lanes):
    return lax.broadcasted_iota(jnp.int32, (rows, lanes), 0) == lax.broadcasted_iota(jnp.int32, (rows, lanes), 1)


def to_row(col, lanes):
    rows = col.shape[0]
    spread = jnp.where(diagonal(rows, lanes), jnp.broadcast_to(col, (rows, lanes)), 0.0)
    return jnp.broadcast_to(jnp.sum(spread, axis=0, keepdims=True), (8, lanes))


def to_col(row, rows):
    lanes = row.shape[1]
    spread = jnp.where(diagonal(rows, lanes), jnp.broadcast_to(row, (rows, lanes)), 0.0)
    return jnp.sum(spread, axis=1, keepdims=True)


def kernel(
    n, chunks, fc, lag, depth,
    tok_ref, gain_ref, gw_ref, gs_ref, uw_ref, us_ref, dw_ref, ds_ref, og_ref,
    out_ref,
    gw, uw, dw, xg, own, rs_send, rs_recv, hid, acc,
    sq1, sq1_send, inv1, pair_send, pair_recv, x_send, x_recv, sq2, fin,
    w_sem, d_sem, rs_ssem, rs_rsem, ag_ssem, ag_rsem,
    sq1_ssem, sq1_rsem, sq2_ssem, sq2_rsem, misc_s, misc_r,
):
    p = lax.axis_index("ra")
    cb = lax.axis_index("cb")
    core = lax.rem(cb, 2)
    partner = cb + 1 - 2 * core
    x_peer = lax.rem(cb + 2, 4)
    toks, dl = tok_ref.shape
    half = toks // 2
    width = dl * n
    last = n - 1

    def w_copy(c, which):
        src, dst = ((gw_ref, gw), (uw_ref, uw))[which]
        cols = pl.ds(pl.multiple_of(c * fc, fc), fc)
        return pltpu.make_async_copy(src.at[:, cols], dst.at[c], w_sem.at[which, c])

    def d_copy(c):
        rows = pl.ds(pl.multiple_of(c * fc, fc), fc)
        return pltpu.make_async_copy(dw_ref.at[rows, :], dw.at[c], d_sem.at[c])

    for c in range(min(depth, chunks)):
        w_copy(c, 0).start()
        w_copy(c, 1).start()

    barrier = pltpu.get_barrier_semaphore()
    for k in range(1, n):
        pl.semaphore_signal(barrier, inc=1, device_id={"ra": lax.rem(p + k, n)}, device_id_type=MESH)
    for other in (partner, x_peer):
        pl.semaphore_signal(barrier, inc=1, device_id={"cb": other}, device_id_type=MESH)

    values = tok_ref[...].astype(F32)
    xg[...] = (values * gain_ref[...]).astype(BF16)
    sq1_send[...] = to_row(jnp.sum(values * values, axis=1, keepdims=True), toks)
    acc[...] = jnp.zeros_like(acc)

    pl.semaphore_wait(barrier, n + 1)

    def sq1_copy(sender, end):
        return pltpu.make_async_remote_copy(
            src_ref=sq1_send, dst_ref=sq1.at[sender],
            send_sem=sq1_ssem.at[0 if end == 0 else 1], recv_sem=sq1_rsem.at[sender],
            device_id={"ra": end}, device_id_type=MESH)

    for end in (0, last):
        @pl.when(p != end)
        def _():
            sq1_copy(p, end).start()

    def owner_of(f):
        return 0 if f == 0 else last

    def toward(f):
        return jnp.maximum(p - 1, 0) if f == 0 else jnp.minimum(p + 1, last)

    def away(f):
        return toward(1 - f)

    def rs_copy(f, c):
        return pltpu.make_async_remote_copy(
            src_ref=rs_send.at[f, c], dst_ref=rs_recv.at[f, c],
            send_sem=rs_ssem.at[f, c], recv_sem=rs_rsem.at[f, c],
            device_id={"ra": toward(f)}, device_id_type=MESH)

    def ag_copy(f, c):
        return pltpu.make_async_remote_copy(
            src_ref=hid.at[f, c], dst_ref=hid.at[f, c],
            send_sem=ag_ssem.at[f, c], recv_sem=ag_rsem.at[f, c],
            device_id={"ra": away(f)}, device_id_type=MESH)

    def down(f, c):
        rows = slice(f * half, (f + 1) * half)
        acc[rows, :] += jnp.dot(hid[f, c], dw[c].astype(BF16), preferred_element_type=F32)

    def step(t, _):
        @pl.when(t < chunks)
        def _():
            w_copy(t, 0).wait()
            w_copy(t, 1).wait()

            @pl.when(t + depth < chunks)
            def _():
                w_copy(t + depth, 0).start()
                w_copy(t + depth, 1).start()

            @pl.when(t == max(min(chunks - depth, last * lag - 1), 0))
            def _():
                def start(c, _):
                    d_copy(c).start()
                    return 0
                lax.fori_loop(0, chunks, start, 0)

            own[t, :, 0:fc] = jnp.dot(xg[...], gw[t].astype(BF16), preferred_element_type=F32)
            own[t, :, fc:2 * fc] = jnp.dot(xg[...], uw[t].astype(BF16), preferred_element_type=F32)

        @pl.when((t == last * lag) & ((p == 0) | (p == last)))
        def _():
            for k in range(1, n):
                sq1_copy(lax.rem(p + k, n), 0).wait_recv()
            total = jnp.zeros((1, toks), F32)
            for k in range(n):
                total += jnp.where(p == k, sq1_send[0:1, :], sq1[k, 0:1, :])
            inv1[...] = jnp.broadcast_to(lax.rsqrt(to_col(total, toks) / width + 1e-06), inv1.shape)

        for f in (0, 1):
            rank = last - p if f == 0 else p
            c = t - rank * lag
            rows = slice(f * half, (f + 1) * half)
            live = (c >= 0) & (c < chunks)

            @pl.when(live & (rank == 0))
            def _():
                rs_send[f, c] = own[c, rows, :].astype(BF16)
                rs_copy(f, c).start()

            @pl.when(live & (rank > 0))
            def _():
                rs_copy(f, c).wait_recv()

            @pl.when(live & (rank > 0) & (rank < last))
            def _():
                rs_send[f, c] = (own[c, rows, :] + rs_recv[f, c].astype(F32)).astype(BF16)
                rs_copy(f, c).start()

            @pl.when(live & (rank == last))
            def _():
                cols = pl.ds(pl.multiple_of(c * fc, fc), fc)
                scale = inv1[rows, 0:1]
                gate = (own[c, rows, 0:fc] + rs_recv[f, c, :, 0:fc].astype(F32)) * scale * gs_ref[:, cols]
                up = (own[c, rows, fc:2 * fc] + rs_recv[f, c, :, fc:2 * fc].astype(F32)) * scale * us_ref[:, cols]
                hid[f, c] = (gate / (1.0 + jnp.exp(-gate)) * up).astype(BF16)
                ag_copy(f, c).start()

        for f in (0, 1):
            rank = p if f == 0 else last - p
            c = t - (last + rank) * lag
            live = (c >= 0) & (c < chunks)

            @pl.when(live & (rank > 0))
            def _():
                ag_copy(f, c).wait_recv()

            @pl.when(live & (rank > 0) & (rank < last))
            def _():
                ag_copy(f, c).start()

            @pl.when(live)
            def _():
                if f == 0:
                    first = rank <= last - rank
                else:
                    first = rank < last - rank

                @pl.when(first)
                def _():
                    d_copy(c).wait()
                down(f, c)

        return 0

    lax.fori_loop(0, chunks + 2 * last * lag, step, 0)

    def misc_copy(src, dst, k, where):
        return pltpu.make_async_remote_copy(
            src_ref=src, dst_ref=dst, send_sem=misc_s.at[k], recv_sem=misc_r.at[k],
            device_id={"cb": where}, device_id_type=MESH)

    mine = pl.ds(pl.multiple_of(core * half, half), half)
    theirs = pl.ds(pl.multiple_of((1 - core) * half, half), half)
    pair_send[...] = acc[theirs, :].astype(BF16)
    to_pair = misc_copy(pair_send, pair_recv, 0, partner)
    to_pair.start()
    to_pair.wait_recv()
    x_send[...] = (acc[mine, :] + pair_recv[...].astype(F32)).astype(BF16)
    to_x = misc_copy(x_send, x_recv, 1, x_peer)
    to_x.start()
    to_x.wait_recv()
    branch = (x_send[...].astype(F32) + x_recv[...].astype(F32)) * ds_ref[...]
    mixed = 0.5 * tok_ref[mine, :].astype(F32) + branch
    acc[mine, :] = mixed
    sq2[n] = to_row(jnp.sum(mixed * mixed, axis=1, keepdims=True), 128)

    def sq2_copy(sender, k):
        return pltpu.make_async_remote_copy(
            src_ref=sq2.at[n], dst_ref=sq2.at[sender],
            send_sem=sq2_ssem.at[k], recv_sem=sq2_rsem.at[sender],
            device_id={"ra": lax.rem(p + k, n)}, device_id_type=MESH)

    for k in range(1, n):
        sq2_copy(p, k).start()
    for k in range(1, n):
        sq2_copy(lax.rem(p + k, n), k).wait_recv()
    total = jnp.zeros((1, 128), F32)
    for k in range(n):
        total += jnp.where(p == k, sq2[n, 0:1, :], sq2[k, 0:1, :])
    inv2 = lax.rsqrt(to_col(total, half) / width + 1e-06)
    fin[0] = (acc[mine, :] * inv2 * og_ref[...]).astype(BF16)
    to_fin = misc_copy(fin.at[0], fin.at[1], 2, partner)
    to_fin.start()
    out_ref[mine, :] = fin[0]
    to_fin.wait_recv()
    out_ref[theirs, :] = fin[1]

    to_pair.wait_send()
    to_x.wait_send()
    to_fin.wait_send()
    for k in range(1, n):
        sq2_copy(p, k).wait_send()
    for end in (0, last):
        @pl.when(p != end)
        def _():
            sq1_copy(p, end).wait_send()
    for f in (0, 1):
        def drain(c, _):
            @pl.when(p != owner_of(f))
            def _():
                rs_copy(f, c).wait_send()

            @pl.when(p != owner_of(1 - f))
            def _():
                ag_copy(f, c).wait_send()
            return 0
        lax.fori_loop(0, chunks, drain, 0)


FC = 256
LAG = 2
DEPTH = 4


def on_device(tokens, norm_gain, gate_weight, gate_scale, up_weight, up_scale, down_weight, down_scale, out_gain):
    n = lax.axis_size("ra")
    toks, dl = tokens.shape
    ff = gate_weight.shape[1]
    half = toks // 2
    need = 12 * dl * ff + 40 * toks * ff
    if n < 2 or lax.axis_size("cb") != 4 or ff % FC or dl % 128 or toks != 128 or need > 56 * 2**20:
        return plain(tokens, norm_gain, gate_weight, gate_scale, up_weight, up_scale, down_weight, down_scale, out_gain)
    chunks = ff // FC
    vmem = pl.BlockSpec(memory_space=pltpu.VMEM)
    hbm = pl.BlockSpec(memory_space=pl.ANY)
    dma = pltpu.SemaphoreType.DMA
    return pl.pallas_call(
        functools.partial(kernel, n, chunks, FC, LAG, DEPTH),
        out_shape=jax.ShapeDtypeStruct((toks, dl), BF16),
        in_specs=[vmem, vmem, hbm, vmem, hbm, vmem, hbm, vmem, vmem],
        out_specs=vmem,
        scratch_shapes=[
            pltpu.VMEM((chunks, dl, FC), F32),
            pltpu.VMEM((chunks, dl, FC), F32),
            pltpu.VMEM((chunks, FC, dl), F32),
            pltpu.VMEM((toks, dl), BF16),
            pltpu.VMEM((chunks, toks, 2 * FC), F32),
            pltpu.VMEM((2, chunks, half, 2 * FC), BF16),
            pltpu.VMEM((2, chunks, half, 2 * FC), BF16),
            pltpu.VMEM((2, chunks, half, FC), BF16),
            pltpu.VMEM((toks, dl), F32),
            pltpu.VMEM((n, 8, toks), F32),
            pltpu.VMEM((8, toks), F32),
            pltpu.VMEM((toks, 128), F32),
            pltpu.VMEM((half, dl), BF16),
            pltpu.VMEM((half, dl), BF16),
            pltpu.VMEM((half, dl), BF16),
            pltpu.VMEM((half, dl), BF16),
            pltpu.VMEM((n + 1, 8, 128), F32),
            pltpu.VMEM((2, half, dl), BF16),
            dma((2, chunks)),
            dma((chunks,)),
            dma((2, chunks)),
            dma((2, chunks)),
            dma((2, chunks)),
            dma((2, chunks)),
            dma((2,)),
            dma((n,)),
            dma((n,)),
            dma((n,)),
            dma((3,)),
            dma((3,)),
        ],
        compiler_params=pltpu.CompilerParams(
            collective_id=0, has_side_effects=True, vmem_limit_bytes=62 * 2**20
        ),
    )(
        tokens, norm_gain[None, :], gate_weight, gate_scale[None, :], up_weight, up_scale[None, :],
        down_weight, down_scale[None, :], out_gain[None, :],
    )


def solution(mesh):
    return jax.shard_map(
        on_device,
        mesh=mesh,
        in_specs=(
            P("grp", "ra"),
            P("ra"),
            P("ra", "cb"),
            P("cb"),
            P("ra", "cb"),
            P("cb"),
            P("cb", "ra"),
            P("ra"),
            P("ra"),
        ),
        out_specs=P("grp", "ra"),
        check_vma=False,
    )
```

time: 174 us -> 62.6 us (0.36)
  waiting for transfers between devices: 89.4 us -> 0 us
  Pallas kernels: 0 us -> 57.9 us
  blocking collectives: 42.3 us -> 0 us
  matrix products: 21.8 us -> 0 us
  between operations: 13.1 us -> 0.01 us
  other arithmetic: 5.53 us -> 0 us
  local copies, waits for them, and re-layouts: 1.56 us -> 4.29 us
    pallas_call x0 -> x1, Pallas kernels: none -> 57.9 us  [on_device(): pl.pallas_call(functools.partial(kernel, n, chunks, FC, LAG, DEPTH), out_...]
    reduce_scatter x2 -> x0, waiting for transfers between devices: 56.8 us -> none  [the longest x1 34.5 us: on_device(): lax.psum_scatter(gate_part, 'ra', scatter_dimension=1, tiled=True)]
    psum x1 -> x0, waiting for transfers between devices: 32.6 us -> none  [on_device(): branch = lax.psum(partial_value, 'cb') * down_scale]
    psum x2 -> x0, blocking collectives: 25.2 us -> none  [the longest x1 13.5 us: on_device(): squares = lax.psum(jnp.sum(values * values, axis=1), 'ra')]
    dot_general x3 -> x0, matrix products: 21.8 us -> none  [the longest x1 7.94 us: on_device(): up_part = jnp.dot(normed_in, up_local, preferred_element_type=jnp.float32)]
    all_gather x1 -> x0, blocking collectives: 17.1 us -> none  [on_device(): lax.all_gather(hidden_share, 'ra', axis=1, tiled=True)]
    convert_element_type x2 -> x0, other arithmetic: 3.21 us -> none  [the longest x1 1.87 us: on_device(): return (mixed * inv_second * out_gain).astype(jnp.bfloat16)]
    broadcast_in_dim x0 -> x2, local copies, waits for them, and re-layouts: none -> 2.62 us  [the longest x1 1.31 us: on_device(): gate_scale[None, :]]
  transfers between devices with their start and end apart: 3 -> 0, of which waited for: 3 -> 0; matrix products, arithmetic and copies ran while one was open for 5% -> 0% of each run, Pallas kernels for 0% -> 0%
where the time goes in v1:
time: 62.6 us; the launch traced here: 62.2 us
  Pallas kernels  57.9 us (92%)
  local copies, waits for them, and re-layouts  4.29 us (7%)
    pallas_call x1, Pallas kernels, on_device(): pl.pallas_call(functools.partial(kernel, n, chunks, FC, LAG, DEPTH), out_...  57.9 us
    unnamed x1, local copies, waits for them, and re-layouts  1.67 us
    broadcast_in_dim x1, local copies, waits for them, and re-layouts, on_device(): gate_scale[None, :]  1.31 us
    broadcast_in_dim x1, local copies, waits for them, and re-layouts, on_device(): up_scale[None, :]  1.31 us

profile of v1, /device:TPU:0, one launch (start us, length us, event | category | flops | bytes accessed | tf_op | source)
XLA Modules:
  0.0 62.2 jit_solution(1751892805665187148)
XLA Ops:
  0.0 1.3 %broadcast_in_dim.16.gs_ref = f32[1,2816]{1,0:T(1,128)} reshape(f32[2816]{0:T(1024)} %param.12) | data formatting | bytes 22528 | tf_op jit(solution)/shard_map/broadcast_in_dim | solution.py:348
  1.3 1.3 %broadcast_in_dim.17.us_ref = f32[1,2816]{1,0:T(1,128)} reshape(f32[2816]{0:T(1024)} %param.14) | data formatting | bytes 22528 | tf_op jit(solution)/shard_map/broadcast_in_dim | solution.py:348
  2.6 57.9 %shard_map.91 = bf16[128,1024]{1,0:T(8,128)(2,1)} custom-call(bf16[128,1024]{1,0:T(8,128)(2,1)} %tok_ref.1, f32[1,1024]{1,0:T(1,128)} %bitcast.3, f32[1024,2816]{1,0:T(8,128)} %gw_ref.1, f32[1,2816]{1,0:T(1,128)} %broadcast_in_dim.16.gs_ref, f32[1024,2816]{1,0:T(8,128)} %uw_ref.1, f32[1,2816]{1,0:T(1,128)} %broadcast_in_dim.17.us_ref, f32[2816,1024]{1,0:T(8,128)} %dw_ref.1, ...), custom_call_target="tpu_custom_call" | custom-call | tf_op jit(solution)/shard_map/pallas_call | solution.py:307
  60.6 1.7 %copy.11 = bf16[128,1024]{1,0:T(8,128)(2,1)} copy(bf16[128,1024]{1,0:T(8,128)(2,1)} %shard_map.91) | data formatting | bytes 524288

commit v2 on v1

--- a/solution.py
+++ b/solution.py
@@ -60,9 +60,9 @@
     tok_ref, gain_ref, gw_ref, gs_ref, uw_ref, us_ref, dw_ref, ds_ref, og_ref,
     out_ref,
     gw, uw, dw, xg, own, rs_send, rs_recv, hid, acc,
-    sq1, sq1_send, inv1, pair_send, pair_recv, x_send, x_recv, sq2, fin,
+    sq1, sq1_send, inv1, scales, pair_send, pair_recv, x_send, x_recv, sq2, fin,
     w_sem, d_sem, rs_ssem, rs_rsem, ag_ssem, ag_rsem,
-    sq1_ssem, sq1_rsem, sq2_ssem, sq2_rsem, misc_s, misc_r,
+    sq1_ssem, sq1_rsem, sq2_ssem, sq2_rsem, misc_s, misc_r, s_sem,
 ):
     p = lax.axis_index("ra")
     cb = lax.axis_index("cb")
@@ -87,6 +87,10 @@
         w_copy(c, 0).start()
         w_copy(c, 1).start()
 
+    s_copies = [pltpu.make_async_copy(ref, scales.at[k, 0], s_sem.at[k]) for k, ref in enumerate((gs_ref, us_ref))]
+    for copy in s_copies:
+        copy.start()
+
     barrier = pltpu.get_barrier_semaphore()
     for k in range(1, n):
         pl.semaphore_signal(barrier, inc=1, device_id={"ra": lax.rem(p + k, n)}, device_id_type=MESH)
@@ -98,6 +102,8 @@
     sq1_send[...] = to_row(jnp.sum(values * values, axis=1, keepdims=True), toks)
     acc[...] = jnp.zeros_like(acc)
 
+    for copy in s_copies:
+        copy.wait()
     pl.semaphore_wait(barrier, n + 1)
 
     def sq1_copy(sender, end):
@@ -190,8 +196,8 @@
             def _():
                 cols = pl.ds(pl.multiple_of(c * fc, fc), fc)
                 scale = inv1[rows, 0:1]
-                gate = (own[c, rows, 0:fc] + rs_recv[f, c, :, 0:fc].astype(F32)) * scale * gs_ref[:, cols]
-                up = (own[c, rows, fc:2 * fc] + rs_recv[f, c, :, fc:2 * fc].astype(F32)) * scale * us_ref[:, cols]
+                gate = (own[c, rows, 0:fc] + rs_recv[f, c, :, 0:fc].astype(F32)) * scale * scales[0, :, cols]
+                up = (own[c, rows, fc:2 * fc] + rs_recv[f, c, :, fc:2 * fc].astype(F32)) * scale * scales[1, :, cols]
                 hid[f, c] = (gate / (1.0 + jnp.exp(-gate)) * up).astype(BF16)
                 ag_copy(f, c).start()
 
@@ -288,8 +294,8 @@
 
 
 FC = 256
-LAG = 2
-DEPTH = 4
+LAG = 4
+DEPTH = 2
 
 
 def on_device(tokens, norm_gain, gate_weight, gate_scale, up_weight, up_scale, down_weight, down_scale, out_gain):
@@ -307,7 +313,7 @@
     return pl.pallas_call(
         functools.partial(kernel, n, chunks, FC, LAG, DEPTH),
         out_shape=jax.ShapeDtypeStruct((toks, dl), BF16),
-        in_specs=[vmem, vmem, hbm, vmem, hbm, vmem, hbm, vmem, vmem],
+        in_specs=[vmem, vmem, hbm, hbm, hbm, hbm, hbm, vmem, vmem],
         out_specs=vmem,
         scratch_shapes=[
             pltpu.VMEM((chunks, dl, FC), F32),
@@ -322,6 +328,7 @@
             pltpu.VMEM((n, 8, toks), F32),
             pltpu.VMEM((8, toks), F32),
             pltpu.VMEM((toks, 128), F32),
+            pltpu.VMEM((2, 1, ff), F32),
             pltpu.VMEM((half, dl), BF16),
             pltpu.VMEM((half, dl), BF16),
             pltpu.VMEM((half, dl), BF16),
@@ -340,12 +347,13 @@
             dma((n,)),
             dma((3,)),
             dma((3,)),
+            dma((2,)),
         ],
         compiler_params=pltpu.CompilerParams(
             collective_id=0, has_side_effects=True, vmem_limit_bytes=62 * 2**20
         ),
     )(
-        tokens, norm_gain[None, :], gate_weight, gate_scale[None, :], up_weight, up_scale[None, :],
+        tokens, norm_gain[None, :], gate_weight, gate_scale, up_weight, up_scale,
         down_weight, down_scale[None, :], out_gain[None, :],
     )
 

time: 62.6 us -> 56.1 us (0.90)
  Pallas kernels: 57.9 us -> 54.2 us
  local copies, waits for them, and re-layouts: 4.29 us -> 1.67 us
    pallas_call x1, Pallas kernels: 57.9 us -> 54.2 us  [on_device(): pl.pallas_call(functools.partial(kernel, n, chunks, FC, LAG, DEPTH), out_...]
    broadcast_in_dim x2 -> x0, local copies, waits for them, and re-layouts: 2.62 us -> none  [the longest x1 1.31 us: on_device(): gate_scale[None, :]]
where the time goes in v2:
time: 56.1 us; the launch traced here: 55.9 us
  Pallas kernels  54.2 us (97%)
  local copies, waits for them, and re-layouts  1.67 us (3%)
    pallas_call x1, Pallas kernels, on_device(): pl.pallas_call(functools.partial(kernel, n, chunks, FC, LAG, DEPTH), out_...  54.2 us
    unnamed x1, local copies, waits for them, and re-layouts  1.67 us

profile of v2, /device:TPU:0, one launch (start us, length us, event | category | flops | bytes accessed | tf_op | source)
XLA Modules:
  0.0 55.9 jit_solution(13959379520501174067)
XLA Ops:
  0.0 54.2 %shard_map.91 = bf16[128,1024]{1,0:T(8,128)(2,1)} custom-call(bf16[128,1024]{1,0:T(8,128)(2,1)} %tok_ref.1, f32[1,1024]{1,0:T(1,128)} %bitcast.3, f32[1024,2816]{1,0:T(8,128)} %gw_ref.1, f32[2816]{0:T(1024)} %gs_ref.1, f32[1024,2816]{1,0:T(8,128)} %uw_ref.1, f32[2816]{0:T(1024)} %us_ref.1, f32[2816,1024]{1,0:T(8,128)} %dw_ref.1, f32[1,1024]{1,0:T(1,128)} %bitcast.4, ...), custom_call_target="tpu_custom_call" | custom-call | tf_op jit(solution)/shard_map/pallas_call | solution.py:313
  54.2 1.7 %copy.11 = bf16[128,1024]{1,0:T(8,128)(2,1)} copy(bf16[128,1024]{1,0:T(8,128)(2,1)} %shard_map.91) | data formatting | bytes 524288

commit v3 on v2

--- a/solution.py
+++ b/solution.py
@@ -57,19 +57,19 @@
 
 def kernel(
     n, chunks, fc, lag, depth,
-    tok_ref, gain_ref, gw_ref, gs_ref, uw_ref, us_ref, dw_ref, ds_ref, og_ref,
-    out_ref,
+    tok_hbm, gain_hbm, gw_ref, gs_ref, uw_ref, us_ref, dw_ref, ds_hbm, og_hbm,
+    out_ref, tok_ref, gain_ref, ds_ref, og_ref,
     gw, uw, dw, xg, own, rs_send, rs_recv, hid, acc,
-    sq1, sq1_send, inv1, scales, pair_send, pair_recv, x_send, x_recv, sq2, fin,
+    sq1, sq1_send, inv1, scales, pair_send, pair_recv, x_send, x_recv, sq2, mixed, fin,
     w_sem, d_sem, rs_ssem, rs_rsem, ag_ssem, ag_rsem,
-    sq1_ssem, sq1_rsem, sq2_ssem, sq2_rsem, misc_s, misc_r, s_sem,
+    sq1_ssem, sq1_rsem, sq2_ssem, sq2_rsem, misc_s, misc_r, s_sem, i_sem,
 ):
     p = lax.axis_index("ra")
     cb = lax.axis_index("cb")
     core = lax.rem(cb, 2)
     partner = cb + 1 - 2 * core
     x_peer = lax.rem(cb + 2, 4)
-    toks, dl = tok_ref.shape
+    toks, dl = tok_hbm.shape
     half = toks // 2
     width = dl * n
     last = n - 1
@@ -83,6 +83,10 @@
         rows = pl.ds(pl.multiple_of(c * fc, fc), fc)
         return pltpu.make_async_copy(dw_ref.at[rows, :], dw.at[c], d_sem.at[c])
 
+    pairs = ((tok_hbm, tok_ref), (gain_hbm, gain_ref), (ds_hbm, ds_ref), (og_hbm, og_ref))
+    i_copies = [pltpu.make_async_copy(a, b, i_sem.at[k]) for k, (a, b) in enumerate(pairs)]
+    for copy in i_copies:
+        copy.start()
     for c in range(min(depth, chunks)):
         w_copy(c, 0).start()
         w_copy(c, 1).start()
@@ -97,6 +101,8 @@
     for other in (partner, x_peer):
         pl.semaphore_signal(barrier, inc=1, device_id={"cb": other}, device_id_type=MESH)
 
+    for copy in i_copies:
+        copy.wait()
     values = tok_ref[...].astype(F32)
     xg[...] = (values * gain_ref[...]).astype(BF16)
     sq1_send[...] = to_row(jnp.sum(values * values, axis=1, keepdims=True), toks)
@@ -214,7 +220,11 @@
             def _():
                 ag_copy(f, c).start()
 
-            @pl.when(live)
+        for f in (0, 1):
+            rank = p if f == 0 else last - p
+            c = t - (last + rank) * lag
+
+            @pl.when((c >= 0) & (c < chunks))
             def _():
                 if f == 0:
                     first = rank <= last - rank
@@ -226,56 +236,81 @@
                     d_copy(c).wait()
                 down(f, c)
 
+        for f in (0, 1):
+            rank = p if f == 0 else last - p
+            t0 = chunks + (last + rank) * lag
+            kept = slice(f * quarter, (f + 1) * quarter)
+
+            @pl.when(t == t0)
+            def _():
+                pair_send[f] = acc[rows_of(f, 1 - core), :].astype(BF16)
+                pair_copy(f).start()
+
+            @pl.when(t == t0 + 2)
+            def _():
+                pair_copy(f).wait_recv()
+                x_send[f] = (acc[rows_of(f, core), :] + pair_recv[f].astype(F32)).astype(BF16)
+                x_copy(f).start()
+
+            @pl.when(t == t0 + 6)
+            def _():
+                x_copy(f).wait_recv()
+                branch = (x_send[f].astype(F32) + x_recv[f].astype(F32)) * ds_ref[...]
+                new = 0.5 * tok_ref[rows_of(f, core), :].astype(F32) + branch
+                mixed[kept, :] = new
+                sq2[f, n] = to_row(jnp.sum(new * new, axis=1, keepdims=True), 128)
+                for k in range(1, n):
+                    sq2_copy(f, p, k).start()
+
         return 0
 
-    lax.fori_loop(0, chunks + 2 * last * lag, step, 0)
+    quarter = half // 2
+
+    def rows_of(f, which):
+        return pl.ds(pl.multiple_of(f * half + which * quarter, quarter), quarter)
 
     def misc_copy(src, dst, k, where):
         return pltpu.make_async_remote_copy(
             src_ref=src, dst_ref=dst, send_sem=misc_s.at[k], recv_sem=misc_r.at[k],
             device_id={"cb": where}, device_id_type=MESH)
 
-    mine = pl.ds(pl.multiple_of(core * half, half), half)
-    theirs = pl.ds(pl.multiple_of((1 - core) * half, half), half)
-    pair_send[...] = acc[theirs, :].astype(BF16)
-    to_pair = misc_copy(pair_send, pair_recv, 0, partner)
-    to_pair.start()
-    to_pair.wait_recv()
-    x_send[...] = (acc[mine, :] + pair_recv[...].astype(F32)).astype(BF16)
-    to_x = misc_copy(x_send, x_recv, 1, x_peer)
-    to_x.start()
-    to_x.wait_recv()
-    branch = (x_send[...].astype(F32) + x_recv[...].astype(F32)) * ds_ref[...]
-    mixed = 0.5 * tok_ref[mine, :].astype(F32) + branch
-    acc[mine, :] = mixed
-    sq2[n] = to_row(jnp.sum(mixed * mixed, axis=1, keepdims=True), 128)
-
-    def sq2_copy(sender, k):
+    def pair_copy(f):
+        return misc_copy(pair_send.at[f], pair_recv.at[f], f, partner)
+
+    def x_copy(f):
+        return misc_copy(x_send.at[f], x_recv.at[f], 2 + f, x_peer)
+
+    def sq2_copy(f, sender, k):
         return pltpu.make_async_remote_copy(
-            src_ref=sq2.at[n], dst_ref=sq2.at[sender],
-            send_sem=sq2_ssem.at[k], recv_sem=sq2_rsem.at[sender],
+            src_ref=sq2.at[f, n], dst_ref=sq2.at[f, sender],
+            send_sem=sq2_ssem.at[f, k], recv_sem=sq2_rsem.at[f, sender],
             device_id={"ra": lax.rem(p + k, n)}, device_id_type=MESH)
 
-    for k in range(1, n):
-        sq2_copy(p, k).start()
-    for k in range(1, n):
-        sq2_copy(lax.rem(p + k, n), k).wait_recv()
-    total = jnp.zeros((1, 128), F32)
-    for k in range(n):
-        total += jnp.where(p == k, sq2[n, 0:1, :], sq2[k, 0:1, :])
-    inv2 = lax.rsqrt(to_col(total, half) / width + 1e-06)
-    fin[0] = (acc[mine, :] * inv2 * og_ref[...]).astype(BF16)
-    to_fin = misc_copy(fin.at[0], fin.at[1], 2, partner)
+    lax.fori_loop(0, chunks + 2 * last * lag + 7, step, 0)
+
+    for f in (0, 1):
+        for k in range(1, n):
+            sq2_copy(f, lax.rem(p + k, n), k).wait_recv()
+        total = jnp.zeros((1, 128), F32)
+        for k in range(n):
+            total += jnp.where(p == k, sq2[f, n, 0:1, :], sq2[f, k, 0:1, :])
+        inv2 = lax.rsqrt(to_col(total, quarter) / width + 1e-06)
+        kept = slice(f * quarter, (f + 1) * quarter)
+        fin[0, kept, :] = (mixed[kept, :] * inv2 * og_ref[...]).astype(BF16)
+    to_fin = misc_copy(fin.at[0], fin.at[1], 4, partner)
     to_fin.start()
-    out_ref[mine, :] = fin[0]
+    for f in (0, 1):
+        out_ref[rows_of(f, core), :] = fin[0, f * quarter:(f + 1) * quarter, :]
     to_fin.wait_recv()
-    out_ref[theirs, :] = fin[1]
-
-    to_pair.wait_send()
-    to_x.wait_send()
+    for f in (0, 1):
+        out_ref[rows_of(f, 1 - core), :] = fin[1, f * quarter:(f + 1) * quarter, :]
+
     to_fin.wait_send()
-    for k in range(1, n):
-        sq2_copy(p, k).wait_send()
+    for f in (0, 1):
+        pair_copy(f).wait_send()
+        x_copy(f).wait_send()
+        for k in range(1, n):
+            sq2_copy(f, p, k).wait_send()
     for end in (0, last):
         @pl.when(p != end)
         def _():
@@ -294,7 +329,7 @@
 
 
 FC = 256
-LAG = 4
+LAG = 3
 DEPTH = 2
 
 
@@ -313,9 +348,13 @@
     return pl.pallas_call(
         functools.partial(kernel, n, chunks, FC, LAG, DEPTH),
         out_shape=jax.ShapeDtypeStruct((toks, dl), BF16),
-        in_specs=[vmem, vmem, hbm, hbm, hbm, hbm, hbm, vmem, vmem],
+        in_specs=[hbm] * 9,
         out_specs=vmem,
         scratch_shapes=[
+            pltpu.VMEM((toks, dl), BF16),
+            pltpu.VMEM((1, dl), F32),
+            pltpu.VMEM((1, dl), F32),
+            pltpu.VMEM((1, dl), F32),
             pltpu.VMEM((chunks, dl, FC), F32),
             pltpu.VMEM((chunks, dl, FC), F32),
             pltpu.VMEM((chunks, FC, dl), F32),
@@ -329,11 +368,12 @@
             pltpu.VMEM((8, toks), F32),
             pltpu.VMEM((toks, 128), F32),
             pltpu.VMEM((2, 1, ff), F32),
-            pltpu.VMEM((half, dl), BF16),
-            pltpu.VMEM((half, dl), BF16),
-            pltpu.VMEM((half, dl), BF16),
-            pltpu.VMEM((half, dl), BF16),
-            pltpu.VMEM((n + 1, 8, 128), F32),
+            pltpu.VMEM((2, half // 2, dl), BF16),
+            pltpu.VMEM((2, half // 2, dl), BF16),
+            pltpu.VMEM((2, half // 2, dl), BF16),
+            pltpu.VMEM((2, half // 2, dl), BF16),
+            pltpu.VMEM((2, n + 1, 8, 128), F32),
+            pltpu.VMEM((half, dl), F32),
             pltpu.VMEM((2, half, dl), BF16),
             dma((2, chunks)),
             dma((chunks,)),
@@ -343,11 +383,12 @@
             dma((2, chunks)),
             dma((2,)),
             dma((n,)),
-            dma((n,)),
-            dma((n,)),
-            dma((3,)),
-            dma((3,)),
+            dma((2, n)),
+            dma((2, n)),
+            dma((5,)),
+            dma((5,)),
             dma((2,)),
+            dma((4,)),
         ],
         compiler_params=pltpu.CompilerParams(
             collective_id=0, has_side_effects=True, vmem_limit_bytes=62 * 2**20

time: 56.1 us -> 55 us (0.980)
  Pallas kernels: 54.2 us -> 53.1 us
    pallas_call x1, Pallas kernels: 54.2 us -> 53.1 us  [on_device(): pl.pallas_call(functools.partial(kernel, n, chunks, FC, LAG, DEPTH), out_...]
where the time goes in v3:
time: 55 us; the launch traced here: 54.8 us
  Pallas kernels  53.1 us (97%)
  local copies, waits for them, and re-layouts  1.67 us (3%)
    pallas_call x1, Pallas kernels, on_device(): pl.pallas_call(functools.partial(kernel, n, chunks, FC, LAG, DEPTH), out_...  53.1 us
    unnamed x1, local copies, waits for them, and re-layouts  1.67 us

profile of v3, /device:TPU:0, one launch (start us, length us, event | category | flops | bytes accessed | tf_op | source)
XLA Modules:
  0.0 54.8 jit_solution(6160761305330346199)
XLA Ops:
  0.0 53.1 %shard_map.91 = bf16[128,1024]{1,0:T(8,128)(2,1)} custom-call(bf16[128,1024]{1,0:T(8,128)(2,1)} %tok_hbm.1, f32[1,1024]{1,0:T(1,128)} %bitcast.3, f32[1024,2816]{1,0:T(8,128)} %gw_ref.1, f32[2816]{0:T(1024)} %gs_ref.1, f32[1024,2816]{1,0:T(8,128)} %uw_ref.1, f32[2816]{0:T(1024)} %us_ref.1, f32[2816,1024]{1,0:T(8,128)} %dw_ref.1, f32[1,1024]{1,0:T(1,128)} %bitcast.4, ...), custom_call_target="tpu_custom_call" | custom-call | tf_op jit(solution)/shard_map/pallas_call | solution.py:348
  53.1 1.7 %copy.11 = bf16[128,1024]{1,0:T(8,128)(2,1)} copy(bf16[128,1024]{1,0:T(8,128)(2,1)} %shard_map.91) | data formatting | bytes 524288
